TPU v7x, 32 devices: a whole 2x2x4 slice. The times are simulated.
32 devices in a mesh: sp: 8 (over z, x), dp: 4 (over y, core).
Axes of the slice: x: 2, y: 2, z: 4, core: 2. Of those that a mesh axis runs over, the one named last changes fastest.
Arguments:
- inputs: bfloat16 [1536, 2048], P('sp'), may hold values from -6 to 6
- w_query: bfloat16 [2048, 2048], P('dp'), may hold values from -0.125 to 0.125
- w_key: bfloat16 [1024, 2048], P('dp'), may hold values from -0.125 to 0.125
- w_value: bfloat16 [1024, 2048], P('dp'), may hold values from -0.125 to 0.125
- query_gain: float32 [64], replicated, may hold values from 0.6 to 7
- key_gain: float32 [64], replicated, may hold values from 0.6 to 7
- grad_out: bfloat16 [1536, 2048], P('sp', 'dp'), may hold values from -6 to 6
Outputs:
- d_inputs: bfloat16 [1536, 2048], P('sp', 'dp')
- grad_wq: float32 [2048, 2048], P('dp')
- grad_wk: float32 [1024, 2048], P('dp')
- grad_wv: float32 [1024, 2048], P('dp')
All inputs are finite; a program needn't handle non-finite values.
Results may differ from a plain program's by a relative error of at most 0.019.
The roundings to bfloat16 on the way count: a program that leaves them out, or rounds other values in their place, can miss the bound.
Values may be sent and summed in bfloat16 or wider, within the bound.
No kernel may reach another device: no remote copies, remote signals or barrier semaphores. Data moves between devices by JAX's collectives and lax.ppermute only.
A program may use at most 64 MiB of HBM per device.

v0:
```python
import jax
import jax.numpy as jnp
from jax import lax
from jax.sharding import PartitionSpec as P

HEAD_WIDTH = 64
GRID_W = 64
norm_eps = 1e-06
axial_base = 10000.0


def rotation_tables(offset, count):
    positions = offset + jnp.arange(count, dtype=jnp.int32)
    grid_rows = (positions // GRID_W).astype(jnp.float32)
    grid_cols = (positions % GRID_W).astype(jnp.float32)
    quarter = HEAD_WIDTH // 4
    freqs_axis = axial_base ** (-jnp.arange(quarter, dtype=jnp.float32) / quarter)
    angle_rows = grid_rows[:, None] * freqs_axis[None, :]
    angle_cols = grid_cols[:, None] * freqs_axis[None, :]
    cosine = jnp.concatenate(
        [jnp.cos(angle_rows), jnp.cos(angle_rows), jnp.cos(angle_cols), jnp.cos(angle_cols)], axis=1
    )
    sine = jnp.concatenate(
        [jnp.sin(angle_rows), jnp.sin(angle_rows), jnp.sin(angle_cols), jnp.sin(angle_cols)], axis=1
    )
    return (cosine, sine)


def quarter_turn(values):
    quarter = HEAD_WIDTH // 4
    return jnp.concatenate(
        [
            -values[..., quarter : 2 * quarter],
            values[..., :quarter],
            -values[..., 3 * quarter :],
            values[..., 2 * quarter : 3 * quarter],
        ],
        axis=-1,
    )


def quarter_back(values):
    quarter = HEAD_WIDTH // 4
    return jnp.concatenate(
        [
            values[..., quarter : 2 * quarter],
            -values[..., :quarter],
            values[..., 3 * quarter :],
            -values[..., 2 * quarter : 3 * quarter],
        ],
        axis=-1,
    )


def rotate(values, cosine, sine):
    return values * cosine + quarter_turn(values) * sine


def rotate_back(grads, cosine, sine):
    return grads * cosine + quarter_back(grads * sine)


def head_norm(raw):
    scale_inv = lax.rsqrt(jnp.mean(raw * raw, axis=-1, keepdims=True) + norm_eps)
    return (raw * scale_inv, scale_inv)


def head_norm_back(grads, normed, scale_inv, gain):
    scaled = grads * gain
    return scale_inv * (scaled - normed * jnp.mean(scaled * normed, axis=-1, keepdims=True))


def body(inputs, w_query, w_key, w_value, query_gain, key_gain, grad_out):
    tok_rows = inputs.shape[0]
    local_query = w_query.shape[0] // HEAD_WIDTH
    local_keys = w_key.shape[0] // HEAD_WIDTH
    group = local_query // local_keys
    key_width = local_keys * HEAD_WIDTH
    scale = HEAD_WIDTH ** (-0.5)
    contract = (((1,), (1,)), ((), ()))
    leading = (((0,), (0,)), ((), ()))
    offset = lax.axis_index("sp") * tok_rows
    cosine, sine = rotation_tables(offset, tok_rows)
    cos_wide = cosine[:, None, :]
    sin_wide = sine[:, None, :]
    q_raw = lax.dot_general(inputs, w_query, contract, preferred_element_type=jnp.float32).astype(
        jnp.bfloat16
    )
    w_pair = jnp.concatenate([w_key, w_value], axis=0)
    kv_raw = lax.dot_general(inputs, w_pair, contract, preferred_element_type=jnp.float32).astype(
        jnp.bfloat16
    )
    q_wide = (
        lax.optimization_barrier(q_raw)
        .astype(jnp.float32)
        .reshape(tok_rows, local_query, HEAD_WIDTH)
    )
    k_wide = (
        lax.optimization_barrier(kv_raw[:, :key_width])
        .astype(jnp.float32)
        .reshape(tok_rows, local_keys, HEAD_WIDTH)
    )
    q_normed, q_inv = head_norm(q_wide)
    k_normed, k_inv = head_norm(k_wide)
    q_rot = rotate(q_normed * query_gain, cos_wide, sin_wide).astype(jnp.bfloat16)
    k_rot = rotate(k_normed * key_gain, cos_wide, sin_wide).astype(jnp.bfloat16)
    kv_rot = jnp.concatenate([k_rot.reshape(tok_rows, key_width), kv_raw[:, key_width:]], axis=1)
    kv_every = lax.all_gather(kv_rot, "sp", axis=0, tiled=True)
    seq_rows = kv_every.shape[0]
    keys_every = kv_every[:, :key_width]
    values_every = kv_every[:, key_width:]
    grad_query = []
    log_totals = []
    deltas = []
    key_terms = [jnp.zeros((seq_rows, HEAD_WIDTH), jnp.float32) for slot in range(local_keys)]
    value_terms = [jnp.zeros((seq_rows, HEAD_WIDTH), jnp.float32) for slot in range(local_keys)]
    for member in range(local_query):
        kv_index = member // group
        query_head = q_rot[:, member, :]
        key_head = keys_every[:, kv_index * HEAD_WIDTH : (kv_index + 1) * HEAD_WIDTH]
        value_head = values_every[:, kv_index * HEAD_WIDTH : (kv_index + 1) * HEAD_WIDTH]
        grad_head = grad_out[:, member * HEAD_WIDTH : (member + 1) * HEAD_WIDTH]
        scores = (
            lax.dot_general(query_head, key_head, contract, preferred_element_type=jnp.float32)
            * scale
        )
        maxima = jnp.max(scores, axis=1, keepdims=True)
        log_total = maxima + jnp.log(jnp.sum(jnp.exp(scores - maxima), axis=1, keepdims=True))
        prob_exact = jnp.exp(scores - log_total)
        prob_half = prob_exact.astype(jnp.bfloat16)
        attn_rows = jnp.dot(prob_half, value_head, preferred_element_type=jnp.float32).astype(
            jnp.bfloat16
        )
        attn_wide = lax.optimization_barrier(attn_rows).astype(jnp.float32)
        delta_rows = jnp.sum(grad_head.astype(jnp.float32) * attn_wide, axis=1, keepdims=True)
        dprob = lax.dot_general(grad_head, value_head, contract, preferred_element_type=jnp.float32)
        dscore = (prob_exact * (dprob - delta_rows)).astype(jnp.bfloat16)
        grad_query.append(jnp.dot(dscore, key_head, preferred_element_type=jnp.float32) * scale)
        log_totals.append(log_total)
        deltas.append(delta_rows)
        value_terms[kv_index] = value_terms[kv_index] + lax.dot_general(
            prob_half, grad_head, leading, preferred_element_type=jnp.float32
        )
        key_terms[kv_index] = (
            key_terms[kv_index]
            + lax.dot_general(dscore, query_head, leading, preferred_element_type=jnp.float32)
            * scale
        )
    gradient_query_rotated = jnp.stack(grad_query, axis=1)
    partial_sums = jnp.concatenate(key_terms + value_terms, axis=1)
    own_grads = lax.psum_scatter(partial_sums, "sp", scatter_dimension=0, tiled=True)
    gradient_key_rotated = own_grads[:, :key_width].reshape(tok_rows, local_keys, HEAD_WIDTH)
    grad_q = head_norm_back(
        rotate_back(gradient_query_rotated, cos_wide, sin_wide), q_normed, q_inv, query_gain
    )
    grad_q = grad_q.reshape(tok_rows, local_query * HEAD_WIDTH).astype(jnp.bfloat16)
    grad_k = head_norm_back(
        rotate_back(gradient_key_rotated, cos_wide, sin_wide), k_normed, k_inv, key_gain
    )
    grad_kv = jnp.concatenate(
        [
            grad_k.reshape(tok_rows, key_width).astype(jnp.bfloat16),
            own_grads[:, key_width:].astype(jnp.bfloat16),
        ],
        axis=1,
    )
    head_part = jnp.dot(grad_q, w_query, preferred_element_type=jnp.float32)
    head_part = head_part + jnp.dot(grad_kv, w_pair, preferred_element_type=jnp.float32)
    d_inputs = lax.psum_scatter(
        head_part.astype(jnp.bfloat16), "dp", scatter_dimension=1, tiled=True
    )
    grad_wq = lax.dot_general(grad_q, inputs, leading, preferred_element_type=jnp.float32)
    grad_wkv = lax.dot_general(grad_kv, inputs, leading, preferred_element_type=jnp.float32)
    grad_wq, grad_wkv = lax.psum((grad_wq, grad_wkv), "sp")
    return (d_inputs, grad_wq, grad_wkv[:key_width], grad_wkv[key_width:])


def solution(mesh):
    return jax.shard_map(
        body,
        mesh=mesh,
        in_specs=(
            P("sp", None),
            P("dp", None),
            P("dp", None),
            P("dp", None),
            P(),
            P(),
            P("sp", "dp"),
        ),
        out_specs=(P("sp", "dp"), P("dp", None), P("dp", None), P("dp", None)),
        check_vma=False,
    )
```

profile of v0, /device:TPU:0, one launch (start us, length us, event | category | flops | bytes accessed | tf_op | source)
XLA Modules:
  0.0 498.9 jit_solution(4581374337283304342)
XLA Ops:
  9.1 1.4 constant_dynamic-update-slice_fusion.1
  16.6 1.7 copy.97
  21.3 1.6 pad_maximum_fusion.1
  22.9 1.5 convolution_convert_fusion.1
  25.2 1.5 copy.126
  26.7 1.5 copy.125
  34.6 35.3 %all-gather.2.cloned.1.call-done = bf16[1536,512]{1,0:T(8,128)(2,1)} async-done(((bf16[192,512]{1,0:T(8,128)(2,1)}), bf16[1536,512]{1,0:T(8,128)(2,1)}) %all-gather.2.cloned.1.call-update) | async-done | bytes 1572880 | tf_op jit(solution)/shard_map/all_gather | solution.py:108
  69.9 1.6 fusion.148
  95.9 1.1 fusion.28
  97.1 1.1 fusion.27
  100.5 3.5 copy.117
  106.2 2.0 copy.109
  108.3 1.6 fusion.53
  109.9 1.6 fusion.51
  111.5 1.7 fusion.49
  116.6 1.6 multiply_reduce_fusion
  118.2 2.0 copy.106
  121.8 1.4 multiply_convert_fusion
  123.2 2.8 fusion.156
  126.0 51.0 %reduce-scatter.7.cloned.1.call-done = f32[192,512]{1,0:T(8,128)} async-done(((f32[1536,512]{1,0:T(8,128)}), f32[192,512]{1,0:T(8,128)}) %reduce-scatter.7.cloned.1.call-update) | async-done | bytes 393232 | tf_op jit(solution)/shard_map/reduce_scatter | solution.py:151
  177.0 1.6 slice.233
  178.6 1.8 copy.112
  181.5 1.6 pad_maximum_fusion
  183.1 1.8 copy.113
  185.7 1.7 copy.114
  188.4 1.3 multiply_convert_fusion.1
  190.3 2.7 fusion.96
  194.8 1.5 fusion.16
  196.3 266.0 %all-reduce.3.cloned.1.call-done = (f32[512,2048]{1,0:T(8,128)}, f32[512,2048]{1,0:T(8,128)}) async-done(((f32[512,2048]{1,0:T(8,128)}, f32[512,2048]{1,0:T(8,128)}), (f32[512,2048]{1,0:T(8,128)}, f32[512,2048]{1,0:T(8,128)})) %all-reduce.3.cloned.1.call-update) | async-done | bytes 8388624 | tf_op jit(solution)/shard_map/psum | solution.py:174
  462.3 4.7 fusion.142
  467.0 20.6 %reduce-scatter.5.cloned.1.call-done = bf16[192,512]{1,0:T(8,128)(2,1)} async-done(((bf16[192,2048]{1,0:T(8,128)(2,1)}), bf16[192,512]{1,0:T(8,128)(2,1)}) %reduce-scatter.5.cloned.1.call-update) | async-done | bytes 196624 | tf_op jit(solution)/shard_map/reduce_scatter | solution.py:169
  487.7 4.7 copy.144
  (222 shorter events, 56.7 us)
Async XLA Ops:
  7.2 15.8 %copy-start = (bf16[512,2048]{1,0:T(8,128)(2,1)S(1)}, bf16[512,2048]{1,0:T(8,128)(2,1)}, u32[]{:S(2)}) copy-start(bf16[512,2048]{1,0:T(8,128)(2,1)} %param.8) | copy-start | bytes 6291460
  7.2 62.7 %all-gather.2.cloned.1.call-start = ((), (), s32[]{:S(2)}) async-start(), calls=%async_computation.2 | async-start | bytes 1769472 | tf_op jit(solution)/shard_map/all_gather | solution.py:108
  8.1 12.0 %copy-start.43 = (f32[256]{0:T(256)}, f32[256]{0:T(256)S(1)}, u32[]{:S(2)}) copy-start(f32[256]{0:T(256)S(1)} %mul.354) | copy-start | bytes 3076
  9.0 107.1 %copy-start.29 = (f32[192,64]{0,1:T(8,128)}, f32[192,64]{0,1:T(8,128)S(1)}, u32[]{:S(2)}) copy-start(f32[192,64]{0,1:T(8,128)S(1)} %pad_maximum_fusion.5) | copy-start | bytes 147460
  9.1 11.0 %copy-start.25 = (f32[192,256]{1,0:T(8,128)}, f32[192,256]{1,0:T(8,128)S(1)}, u32[]{:S(2)}) copy-start(f32[192,256]{1,0:T(8,128)S(1)} %copy.96) | copy-start | bytes 589828
  9.1 1.6 copy-start.30
  10.7 1.1 copy-start.3
  11.9 1.3 copy-start.19
  11.9 3.1 copy-start.48
  14.9 3.5 copy-start.21
  20.1 2.7 copy-start.27
  22.9 1.6 copy-start.4
  22.9 154.1 %reduce-scatter.7.cloned.1.call-start = ((), (), s32[]{:S(2)}) async-start(), calls=%async_computation.4 | async-start | bytes 3538944 | tf_op jit(solution)/shard_map/reduce_scatter | solution.py:151
  24.5 9.1 %copy-start.45 = (f32[64]{0:T(128)S(1)}, f32[64]{0:T(128)}, u32[]{:S(2)}) copy-start(f32[64]{0:T(128)} %param.11) | copy-start | bytes 772
  69.9 1.9 copy-start.1
  94.9 2.1 copy-start.12
  104.0 358.3 %all-reduce.3.cloned.1.call-start = ((), (), s32[]{:S(2)}) async-start(), calls=%async_computation.5 | async-start | bytes 16777216 | tf_op jit(solution)/shard_map/psum | solution.py:174
  108.3 3.2 copy-start.2
  109.9 3.3 copy-start.17
  111.5 2.2 copy-start.9
  113.7 1.1 copy-start.7
  114.2 1.1 copy-start.13
  118.1 3.7 copy-start.47
  126.0 55.5 %copy-start.22 = (f32[192,256]{0,1:T(8,128)S(1)}, f32[192,256]{0,1:T(8,128)}, u32[]{:S(2)}) copy-start(f32[192,256]{0,1:T(8,128)} %copy-done.21) | copy-start | bytes 589828
  126.0 55.5 %copy-start.49 = (f32[64]{0:T(128)S(1)}, f32[64]{0:T(128)}, u32[]{:S(2)}) copy-start(f32[64]{0:T(128)} %param.12) | copy-start | bytes 772
  180.4 1.1 copy-start.24
  181.5 6.8 %copy-start.26 = (f32[192,256]{1,0:T(8,128)S(1)}, f32[192,256]{1,0:T(8,128)}, u32[]{:S(2)}) copy-start(f32[192,256]{1,0:T(8,128)} %copy-done.25) | copy-start | bytes 589828
  181.5 6.8 %copy-start.44 = (f32[256]{0:T(256)S(1)}, f32[256]{0:T(256)}, u32[]{:S(2)}) copy-start(f32[256]{0:T(256)} %copy-done.43) | copy-start | bytes 3076
  183.1 5.2 %copy-start.28 = (f32[192,256]{1,0:T(8,128)S(1)}, f32[192,256]{1,0:T(8,128)}, u32[]{:S(2)}) copy-start(f32[192,256]{1,0:T(8,128)} %copy-done.27) | copy-start | bytes 589828
  188.4 1.3 copy-start.31
  193.1 294.6 %reduce-scatter.5.cloned.1.call-start = ((), (), s32[]{:S(2)}) async-start(), calls=%async_computation.3 | async-start | bytes 983040 | tf_op jit(solution)/shard_map/reduce_scatter | solution.py:169
  193.1 1.6 copy-start.20
  (22 other events, 18.5 us)
Sparse Core Ops, SparseCore 0:
  23.0 46.8 all-gather.1
  104.2 72.8 reduce-scatter.6
  193.2 269.0 all-reduce.2
  465.3 22.3 reduce-scatter.4
where the time goes:
time: 500 us; the launch traced here: 499 us
  waiting for transfers between devices  373 us (75%)
  local copies, waits for them, and re-layouts  54.1 us (11%)
  matrix products  40.2 us (8%)
  other arithmetic  16.9 us (3%)
  between operations  14.6 us (3%)
    psum x1, waiting for transfers between devices, body(): grad_wq, grad_wkv = lax.psum((grad_wq, grad_wkv), 'sp')  266 us
    reduce_scatter x1, waiting for transfers between devices, body(): lax.psum_scatter(partial_sums, 'sp', scatter_dimension=0, tiled=True)  51 us
    all_gather x1, waiting for transfers between devices, body(): kv_every = lax.all_gather(kv_rot, 'sp', axis=0, tiled=True)  35.3 us
    unnamed x112, local copies, waits for them, and re-layouts  26.3 us
    reduce_scatter x1, waiting for transfers between devices, body(): lax.psum_scatter(head_part.astype(jnp.bfloat16), 'dp', scatter_dimension=...  20.6 us
  transfers between devices with their start and end apart: 4, of which 4 were waited for; matrix products, arithmetic and copies ran while one was open for 8% of the time, Pallas kernels for 0%

commit v1 on v0

--- a/solution.py
+++ b/solution.py
@@ -105,7 +105,21 @@
     q_rot = rotate(q_normed * query_gain, cos_wide, sin_wide).astype(jnp.bfloat16)
     k_rot = rotate(k_normed * key_gain, cos_wide, sin_wide).astype(jnp.bfloat16)
     kv_rot = jnp.concatenate([k_rot.reshape(tok_rows, key_width), kv_raw[:, key_width:]], axis=1)
-    kv_every = lax.all_gather(kv_rot, "sp", axis=0, tiled=True)
+    ways, here, step = (lax.axis_size("sp"), lax.axis_index("sp"), kv_rot.shape[0])
+    dims = [n * ways if d == 0 else n for d, n in enumerate(kv_rot.shape)]
+    full = lax.dynamic_update_slice_in_dim(
+        jnp.zeros(dims, kv_rot.dtype), kv_rot, here * step, axis=0
+    )
+    going_up = going_down = kv_rot
+    for far in range(1, ways // 2 + 1):
+        going_up = lax.ppermute(going_up, "sp", [(d, (d + 1) % ways) for d in range(ways)])
+        full = lax.dynamic_update_slice_in_dim(full, going_up, (here - far) % ways * step, axis=0)
+        if 2 * far < ways:
+            going_down = lax.ppermute(going_down, "sp", [(d, (d - 1) % ways) for d in range(ways)])
+            full = lax.dynamic_update_slice_in_dim(
+                full, going_down, (here + far) % ways * step, axis=0
+            )
+    kv_every = full
     seq_rows = kv_every.shape[0]
     keys_every = kv_every[:, :key_width]
     values_every = kv_every[:, key_width:]

time: 500 us -> 518 us (1.036)
  waiting for transfers between devices: 373 us -> 342 us
  matrix products: 40.2 us -> 68.4 us
  starting transfers between devices: 0.16 us -> 18.6 us
    all_gather x1 -> x0, waiting for transfers between devices: 35.3 us -> none  [body(): kv_every = lax.all_gather(kv_rot, 'sp', axis=0, tiled=True)]
    ppermute x0 -> x7, starting transfers between devices: none -> 18.5 us  [the longest x3 11.3 us: body(): lax.ppermute(going_down, 'sp', [(d, (d - 1) % ways) for d in range(ways)])]
    ppermute x0 -> x7, waiting for transfers between devices: none -> 8.64 us  [the longest x4 8.63 us: body(): lax.ppermute(going_up, 'sp', [(d, (d + 1) % ways) for d in range(ways)])]
    dot_general x8, matrix products: 3.17 us -> 11.6 us  [body(): lax.dot_general(grad_head, value_head, contract, preferred_element_type=j...]
    dot_general x8, matrix products: 3.8 us -> 11.8 us  [body(): jnp.dot(prob_half, value_head, preferred_element_type=jnp.float32)]
    unnamed x112 -> x110, local copies, waits for them, and re-layouts: 26.3 us -> 19.4 us
    dot_general x8, matrix products: 5.09 us -> 12 us  [body(): lax.dot_general(query_head, key_head, contract, preferred_element_type=jn...]
    dynamic_update_slice x0 -> x7, local copies, waits for them, and re-layouts: none -> 6.68 us  [the longest x4 3.68 us: body(): lax.dynamic_update_slice_in_dim(full, going_up, (here - far) % ways * ste...]
  transfers between devices with their start and end apart: 4 -> 10, of which waited for: 4 -> 6; matrix products, arithmetic and copies ran while one was open for 8% -> 10% of each run, Pallas kernels for 0% -> 0%
where the time goes in v1:
time: 518 us; the launch traced here: 516 us
  waiting for transfers between devices  342 us (66%)
  matrix products  68.4 us (13%)
  local copies, waits for them, and re-layouts  55.2 us (11%)
  starting transfers between devices  18.6 us (4%)
  other arithmetic  17.2 us (3%)
  between operations  14.7 us (3%)
    psum x1, waiting for transfers between devices, body(): grad_wq, grad_wkv = lax.psum((grad_wq, grad_wkv), 'sp')  266 us
    reduce_scatter x1, waiting for transfers between devices, body(): lax.psum_scatter(partial_sums, 'sp', scatter_dimension=0, tiled=True)  46.2 us
    reduce_scatter x1, waiting for transfers between devices, body(): lax.psum_scatter(head_part.astype(jnp.bfloat16), 'dp', scatter_dimension=...  20.8 us
    unnamed x110, local copies, waits for them, and re-layouts  19.4 us
    dot_general x8, matrix products, body(): jnp.dot(dscore, key_head, preferred_element_type=jnp.float32) * scale  12.3 us
    dot_general x8, matrix products, body(): lax.dot_general(query_head, key_head, contract, preferred_element_type=jn...  12 us
    dot_general x8, matrix products, body(): jnp.dot(prob_half, value_head, preferred_element_type=jnp.float32)  11.8 us
    dot_general x8, matrix products, body(): lax.dot_general(grad_head, value_head, contract, preferred_element_type=j...  11.6 us
  transfers between devices with their start and end apart: 10, of which 6 were waited for; matrix products, arithmetic and copies ran while one was open for 10% of the time, Pallas kernels for 0%

profile of v1, /device:TPU:0, one launch (start us, length us, event | category | flops | bytes accessed | tf_op | source)
XLA Modules:
  0.0 515.8 jit_solution(12537165987026961216)
XLA Ops:
  16.6 1.7 copy.97
  23.3 3.0 collective-permute-start
  26.3 3.0 collective-permute-start.1
  40.0 4.7 collective-permute-start.3
  44.7 1.6 constant_dynamic-update-slice_fusion.8
  46.3 1.6 constant_dynamic-update-slice_fusion.7
  49.3 1.7 collective-permute-start.4
  51.0 3.5 collective-permute-start.5
  55.9 2.6 collective-permute-done.4
  58.5 2.5 collective-permute-start.6
  62.4 4.6 collective-permute-done.6
  101.6 1.6 fusion.18
  106.9 1.6 fusion.24
  117.2 3.5 copy.117
  123.0 2.0 copy.109
  125.0 1.7 fusion.53
  128.3 1.6 fusion.49
  129.9 1.6 fusion.47
  138.1 1.6 multiply_reduce_fusion
  139.7 2.0 copy.106
  144.8 2.8 fusion.156
  147.5 46.2 %reduce-scatter.7.cloned.1.call-done = f32[192,512]{1,0:T(8,128)} async-done(((f32[1536,512]{1,0:T(8,128)}), f32[192,512]{1,0:T(8,128)}) %reduce-scatter.7.cloned.1.call-update) | async-done | bytes 393232 | tf_op jit(solution)/shard_map/reduce_scatter | solution.py:165
  193.7 1.6 slice.233
  195.3 1.8 copy.112
  198.2 1.6 pad_maximum_fusion
  199.8 1.8 copy.113
  202.4 1.7 copy.114
  207.1 2.7 fusion.96
  213.1 266.0 %all-reduce.3.cloned.1.call-done = (f32[512,2048]{1,0:T(8,128)}, f32[512,2048]{1,0:T(8,128)}) async-done(((f32[512,2048]{1,0:T(8,128)}, f32[512,2048]{1,0:T(8,128)}), (f32[512,2048]{1,0:T(8,128)}, f32[512,2048]{1,0:T(8,128)})) %all-reduce.3.cloned.1.call-update) | async-done | bytes 8388624 | tf_op jit(solution)/shard_map/psum | solution.py:188
  479.1 4.7 fusion.142
  483.8 20.8 %reduce-scatter.5.cloned.1.call-done = bf16[192,512]{1,0:T(8,128)(2,1)} async-done(((bf16[192,2048]{1,0:T(8,128)(2,1)}), bf16[192,512]{1,0:T(8,128)(2,1)}) %reduce-scatter.5.cloned.1.call-update) | async-done | bytes 196624 | tf_op jit(solution)/shard_map/reduce_scatter | solution.py:183
  504.5 4.7 copy.152
  (239 shorter events, 96.9 us)
Async XLA Ops:
  7.2 22.2 %copy-start = (bf16[512,2048]{1,0:T(8,128)(2,1)S(1)}, bf16[512,2048]{1,0:T(8,128)(2,1)}, u32[]{:S(2)}) copy-start(bf16[512,2048]{1,0:T(8,128)(2,1)} %param.8) | copy-start | bytes 6291460
  7.2 186.5 %reduce-scatter.7.cloned.1.call-start = ((), (), s32[]{:S(2)}) async-start(), calls=%async_computation.3 | async-start | bytes 3538944 | tf_op jit(solution)/shard_map/reduce_scatter | solution.py:165
  8.1 12.0 %copy-start.42 = (f32[256]{0:T(256)}, f32[256]{0:T(256)S(1)}, u32[]{:S(2)}) copy-start(f32[256]{0:T(256)S(1)} %mul.376) | copy-start | bytes 3076
  9.0 128.6 %copy-start.27 = (f32[192,64]{0,1:T(8,128)}, f32[192,64]{0,1:T(8,128)S(1)}, u32[]{:S(2)}) copy-start(f32[192,64]{0,1:T(8,128)S(1)} %pad_maximum_fusion.5) | copy-start | bytes 147460
  9.1 11.0 %copy-start.23 = (f32[192,256]{1,0:T(8,128)}, f32[192,256]{1,0:T(8,128)S(1)}, u32[]{:S(2)}) copy-start(f32[192,256]{1,0:T(8,128)S(1)} %copy.96) | copy-start | bytes 589828
  11.9 3.1 copy-start.47
  14.9 3.5 copy-start.20
  23.3 16.6 %collective-permute-start = (bf16[192,512]{1,0:T(8,128)(2,1)}, bf16[192,512]{1,0:T(8,128)(2,1)}, u32[]{:S(2)}, u32[]{:S(2)}) collective-permute-start(bf16[192,512]{1,0:T(8,128)(2,1)} %get-tuple-element.36), channel_id=1, source_target_pairs={{0,4},{4,8},{8,12},{12,16},{16,20},{20,24},{24,28},{28,0},{1,5},{5... | collective-permute-start | bytes 589832 | tf_op jit(solution)/shard_map/ppermute | solution.py:115
  26.3 13.7 %collective-permute-start.1 = (bf16[192,512]{1,0:T(8,128)(2,1)}, bf16[192,512]{1,0:T(8,128)(2,1)}, u32[]{:S(2)}, u32[]{:S(2)}) collective-permute-start(bf16[192,512]{1,0:T(8,128)(2,1)} %get-tuple-element.36), channel_id=1, source_target_pairs={{0,28},{4,0},{8,4},{12,8},{16,12},{20,16},{24,20},{28,24},{1,29},{... | collective-permute-start | bytes 589832 | tf_op jit(solution)/shard_map/ppermute | solution.py:118
  30.9 6.8 %copy-start.44 = (f32[64]{0:T(128)S(1)}, f32[64]{0:T(128)}, u32[]{:S(2)}) copy-start(f32[64]{0:T(128)} %param.11) | copy-start | bytes 772
  39.9 9.4 %collective-permute-start.2 = (bf16[192,512]{1,0:T(8,128)(2,1)}, bf16[192,512]{1,0:T(8,128)(2,1)S(1)}, u32[]{:S(2)}, u32[]{:S(2)}) collective-permute-start(bf16[192,512]{1,0:T(8,128)(2,1)} %collective-permute-done), channel_id=1, source_target_pairs={{0,4},{4,8},{8,12},{12,16},{16,20},{20,24},{24,28},{28,0},{1,5},{5... | collective-permute-start | bytes 589832 | tf_op jit(solution)/shard_map/ppermute | solution.py:115
  40.0 11.1 %collective-permute-start.3 = (bf16[192,512]{1,0:T(8,128)(2,1)}, bf16[192,512]{1,0:T(8,128)(2,1)S(1)}, u32[]{:S(2)}, u32[]{:S(2)}) collective-permute-start(bf16[192,512]{1,0:T(8,128)(2,1)} %collective-permute-done.1), channel_id=1, source_target_pairs={{0,28},{4,0},{8,4},{12,8},{16,12},{20,16},{24,20},{28,24},{1,29},{... | collective-permute-start | bytes 589832 | tf_op jit(solution)/shard_map/ppermute | solution.py:118
  49.3 9.2 %collective-permute-start.4 = (bf16[192,512]{1,0:T(8,128)(2,1)S(1)}, bf16[192,512]{1,0:T(8,128)(2,1)S(1)}, u32[]{:S(2)}, u32[]{:S(2)}) collective-permute-start(bf16[192,512]{1,0:T(8,128)(2,1)S(1)} %collective-permute-done.2), channel_id=1, source_target_pairs={{0,4},{4,8},{8,12},{12,16},{16,20},{20,24},{24,28},{28,0},{1,5},{5... | collective-permute-start | bytes 589832 | tf_op jit(solution)/shard_map/ppermute | solution.py:115
  51.0 10.7 %collective-permute-start.5 = (bf16[192,512]{1,0:T(8,128)(2,1)S(1)}, bf16[192,512]{1,0:T(8,128)(2,1)S(1)}, u32[]{:S(2)}, u32[]{:S(2)}) collective-permute-start(bf16[192,512]{1,0:T(8,128)(2,1)S(1)} %collective-permute-done.3), channel_id=1, source_target_pairs={{0,28},{4,0},{8,4},{12,8},{16,12},{20,16},{24,20},{28,24},{1,29},{... | collective-permute-start | bytes 589832 | tf_op jit(solution)/shard_map/ppermute | solution.py:118
  58.5 8.5 %collective-permute-start.6 = (bf16[192,512]{1,0:T(8,128)(2,1)S(1)}, bf16[192,512]{1,0:T(8,128)(2,1)S(1)}, u32[]{:S(2)}, u32[]{:S(2)}) collective-permute-start(bf16[192,512]{1,0:T(8,128)(2,1)S(1)} %collective-permute-done.4), channel_id=1, source_target_pairs={{0,4},{4,8},{8,12},{12,16},{16,20},{20,24},{24,28},{28,0},{1,5},{5... | collective-permute-start | bytes 589832 | tf_op jit(solution)/shard_map/ppermute | solution.py:115
  91.6 17.1 %copy-start.11 = (bf16[192,1536]{1,0:T(8,128)(2,1)}, bf16[192,1536]{1,0:T(8,128)(2,1)S(1)}, u32[]{:S(2)}) copy-start(bf16[192,1536]{1,0:T(8,128)(2,1)S(1)} %fusion.23) | copy-start | bytes 1769476
  95.0 14.7 %copy-start.12 = (bf16[192,1536]{1,0:T(8,128)(2,1)}, bf16[192,1536]{1,0:T(8,128)(2,1)S(1)}, u32[]{:S(2)}) copy-start(bf16[192,1536]{1,0:T(8,128)(2,1)S(1)} %fusion.21) | copy-start | bytes 1769476
  98.2 12.5 %copy-start.14 = (bf16[192,1536]{1,0:T(8,128)(2,1)}, bf16[192,1536]{1,0:T(8,128)(2,1)S(1)}, u32[]{:S(2)}) copy-start(bf16[192,1536]{1,0:T(8,128)(2,1)S(1)} %fusion.19) | copy-start | bytes 1769476
  101.6 10.1 %copy-start.16 = (bf16[192,1536]{1,0:T(8,128)(2,1)}, bf16[192,1536]{1,0:T(8,128)(2,1)S(1)}, u32[]{:S(2)}) copy-start(bf16[192,1536]{1,0:T(8,128)(2,1)S(1)} %fusion.17) | copy-start | bytes 1769476
  120.7 358.3 %all-reduce.3.cloned.1.call-start = ((), (), s32[]{:S(2)}) async-start(), calls=%async_computation.4 | async-start | bytes 16777216 | tf_op jit(solution)/shard_map/psum | solution.py:188
  125.0 3.3 copy-start.9
  126.7 3.2 copy-start.13
  128.3 3.2 copy-start.7
  129.9 3.0 copy-start.15
  132.9 3.0 copy-start.17
  139.7 3.7 copy-start.46
  147.5 50.7 %copy-start.21 = (f32[192,256]{0,1:T(8,128)S(1)}, f32[192,256]{0,1:T(8,128)}, u32[]{:S(2)}) copy-start(f32[192,256]{0,1:T(8,128)} %copy-done.20) | copy-start | bytes 589828
  147.5 50.7 %copy-start.48 = (f32[64]{0:T(128)S(1)}, f32[64]{0:T(128)}, u32[]{:S(2)}) copy-start(f32[64]{0:T(128)} %param.12) | copy-start | bytes 772
  198.2 6.9 %copy-start.24 = (f32[192,256]{1,0:T(8,128)S(1)}, f32[192,256]{1,0:T(8,128)}, u32[]{:S(2)}) copy-start(f32[192,256]{1,0:T(8,128)} %copy-done.23) | copy-start | bytes 589828
  198.2 6.9 %copy-start.43 = (f32[256]{0:T(256)S(1)}, f32[256]{0:T(256)}, u32[]{:S(2)}) copy-start(f32[256]{0:T(256)} %copy-done.42) | copy-start | bytes 3076
  199.8 5.3 %copy-start.26 = (f32[192,256]{1,0:T(8,128)S(1)}, f32[192,256]{1,0:T(8,128)}, u32[]{:S(2)}) copy-start(f32[192,256]{1,0:T(8,128)} %copy-done.25) | copy-start | bytes 589828
  209.8 294.7 %reduce-scatter.5.cloned.1.call-start = ((), (), s32[]{:S(2)}) async-start(), calls=%async_computation.2 | async-start | bytes 983040 | tf_op jit(solution)/shard_map/reduce_scatter | solution.py:183
  (27 other events, 42.6 us)
Sparse Core Ops, SparseCore 0:
  120.9 72.8 reduce-scatter.6
  209.9 269.0 all-reduce.2
  482.2 22.3 reduce-scatter.4
